TPU v7x, 128 devices: a whole 4x4x4 slice. The times are simulated.
128 devices in a mesh: fs: 16 (over z, x), tp: 8 (over y, core).
Axes of the slice: x: 4, y: 4, z: 4, core: 2. Of those that a mesh axis runs over, the one named last changes fastest.
Arguments:
- normed_input: bfloat16 [32768, 2048], P('fs'), may hold values from -6 to 6
- forget_cot: bfloat16 [32768, 2048], P('fs', 'tp'), may hold values from -6 to 6
- value_cot: bfloat16 [32768, 2048], P('fs', 'tp'), may hold values from -6 to 6
- gated_output: bfloat16 [32768, 2048], P('fs', 'tp'), may hold values from -6 to 6
- output_cot: bfloat16 [32768, 2048], P('fs'), may hold values from -6 to 6
- forget_weight: float32 [2048, 2048], P('fs', 'tp'), may hold values from -0.125 to 0.125
- value_weight: float32 [2048, 2048], P('fs', 'tp'), may hold values from -0.125 to 0.125
- out_weight: float32 [2048, 2048], P('tp', 'fs'), may hold values from -0.125 to 0.125
- bases: bfloat16 [3, 2048, 256], replicated, may hold values from -0.125 to 0.125
- first_moment: float32 [256, 3, 2048], P('fs', None, 'tp'), may hold values from -4 to 4
- second_moment: float32 [256, 3, 2048], P('fs', None, 'tp'), may hold values from 0.25 to 4
Outputs:
- new_forget: float32 [2048, 2048], P('fs', 'tp')
- new_value: float32 [2048, 2048], P('fs', 'tp')
- new_out: float32 [2048, 2048], P('tp', 'fs')
- copy_forget: bfloat16 [2048, 2048], P(None, 'tp')
- copy_value: bfloat16 [2048, 2048], P(None, 'tp')
- copy_out: bfloat16 [2048, 2048], P('tp')
- moment_one: float32 [256, 3, 2048], P('fs', None, 'tp')
- moment_two: float32 [256, 3, 2048], P('fs', None, 'tp')
- step_forget: float32 [2048, 2048], P('fs', 'tp')
- step_value: float32 [2048, 2048], P('fs', 'tp')
- step_out: float32 [2048, 2048], P('tp', 'fs')
All inputs are finite; a program needn't handle non-finite values.
Results may differ from a plain program's by a relative error of at most 0.0045.
Values may be sent and summed in bfloat16 or wider, within the bound.
No kernel may reach another device: no remote copies, remote signals or barrier semaphores. Data moves between devices by JAX's collectives and lax.ppermute only.
A program may use at most 128 MiB of HBM per device.

v0:
```python
import functools
import jax
import jax.numpy as jnp
from jax import lax
from jax.sharding import Mesh
from jax.sharding import PartitionSpec as P

FS = ("fs_0", "fs_1")
FS_TP = ("fs_0", "fs_1", "tp_0", "tp_1")
TP = ("tp_0", "tp_1")


def in_blocks(value, dim, count):
    before, after = (value.shape[:dim], value.shape[dim + 1 :])
    return jnp.moveaxis(value.reshape(*before, count, -1, *after), dim, 0)


def sum_at_owner(value, axis, dim):
    pieces = in_blocks(value, dim, lax.axis_size(axis))
    arrived = lax.all_to_all(pieces, axis, split_axis=0, concat_axis=0, tiled=True)
    return arrived.astype(jnp.float32).sum(axis=0)


def joined_along(pieces, dim):
    dims = list(pieces.shape[1:])
    dims[dim] *= pieces.shape[0]
    return jnp.moveaxis(pieces, 0, dim).reshape(dims)


def sent_to_all(value, axis):
    copies = jnp.broadcast_to(value, (lax.axis_size(axis), *value.shape))
    return lax.all_to_all(copies, axis, split_axis=0, concat_axis=0, tiled=True)


def gather_directly(value, axis, dim):
    return joined_along(sent_to_all(value, axis), dim)


def over_axes(value, axes):
    return functools.reduce(lax.psum, axes, value)


def gather_turned(arrays, axis, dims):
    turned = [jnp.moveaxis(a, dim, 0) for a, dim in zip(arrays, dims)]
    both = jnp.concatenate([t.reshape(len(t), -1) for t in turned], axis=1)
    result, at, finished = (lax.all_gather(both, axis, axis=0, tiled=True), 0, [])
    for t, dim in zip(turned, dims):
        piece = result[:, at : at + t[0].size].reshape(-1, *t.shape[1:])
        finished.append(jnp.moveaxis(piece, 0, dim))
        at += t[0].size
    return tuple(finished)


def split_parts(values):
    high = lax.optimization_barrier(values.astype(jnp.bfloat16))
    low = (values - high.astype(jnp.float32)).astype(jnp.bfloat16)
    return (high, low)


def on_device(
    normed_input,
    forget_cot,
    value_cot,
    gated_output,
    output_cot,
    forget_weight,
    value_weight,
    out_weight,
    bases,
    first_moment,
    second_moment,
):
    rows = forget_weight.shape[0]
    rank_rows = first_moment.shape[0]
    columns = forget_weight.shape[1]
    offset = lax.axis_index(FS) * rows
    factor = float(normed_input.shape[0] * lax.axis_size(FS)) ** (-0.5)
    my_bases = lax.dynamic_slice_in_dim(bases, offset, rows, 1)
    reduced = jnp.stack(
        [
            jnp.dot(normed_input, bases[0], preferred_element_type=jnp.float32),
            jnp.dot(normed_input, bases[1], preferred_element_type=jnp.float32),
            jnp.dot(output_cot, bases[2], preferred_element_type=jnp.float32),
        ],
        axis=1,
    )
    reduced_high, reduced_low = split_parts(reduced)
    paired = jnp.stack([forget_cot, value_cot, gated_output], axis=1)
    upper = jnp.einsum("tkr,tkc->rkc", reduced_high, paired, preferred_element_type=jnp.float32)
    lower = jnp.einsum("tkr,tkc->rkc", reduced_low, paired, preferred_element_type=jnp.float32)
    projected = sum_at_owner(((upper + lower) * factor).astype(jnp.bfloat16), FS, 0)
    moment_one = 0.9 * first_moment + 0.1 * projected
    moment_two = 0.9 * second_moment + 0.1 * projected * projected
    direction = moment_one / (jnp.sqrt(moment_two) + 1e-08)
    piece_high, piece_low = split_parts(gather_directly(direction, FS, 0))
    upper = jnp.einsum("kdr,rkc->dkc", my_bases, piece_high, preferred_element_type=jnp.float32)
    lower = jnp.einsum("kdr,rkc->dkc", my_bases, piece_low, preferred_element_type=jnp.float32)
    full = upper + lower
    totals = over_axes(jnp.sum(direction * direction, axis=(0, 2)), FS_TP)
    entries = rank_rows * lax.axis_size(FS) * columns * lax.axis_size(TP)
    scale = lax.rsqrt(totals / entries + 1.0)
    full = full * scale[None, :, None]
    step_forget = full[:, 0, :]
    step_value = full[:, 1, :]
    step_out = full[:, 2, :].T
    new_forget = forget_weight - 0.01 * step_forget
    new_value = value_weight - 0.01 * step_value
    new_out = out_weight - 0.01 * step_out
    copy_forget, copy_value, copy_out = gather_turned(
        (
            new_forget.astype(jnp.bfloat16),
            new_value.astype(jnp.bfloat16),
            new_out.astype(jnp.bfloat16),
        ),
        FS,
        (0, 0, 1),
    )
    return (
        new_forget,
        new_value,
        new_out,
        copy_forget,
        copy_value,
        copy_out,
        moment_one,
        moment_two,
        step_forget,
        step_value,
        step_out,
    )


def solution(mesh):
    torus = Mesh(mesh.devices.reshape(4, 4, 4, 2), ("fs_0", "fs_1", "tp_0", "tp_1"))
    placed = (
        P(FS, None),
        P(FS, TP),
        P(FS, TP),
        P(FS, TP),
        P(FS, None),
        P(FS, TP),
        P(FS, TP),
        P(TP, FS),
        P(),
        P(FS, None, TP),
        P(FS, None, TP),
    )
    return jax.shard_map(
        on_device,
        mesh=torus,
        in_specs=placed,
        out_specs=(
            P(FS, TP),
            P(FS, TP),
            P(TP, FS),
            P(None, TP),
            P(None, TP),
            P(TP, None),
            P(FS, None, TP),
            P(FS, None, TP),
            P(FS, TP),
            P(FS, TP),
            P(TP, FS),
        ),
        check_vma=False,
    )
```

profile of v0, /device:TPU:0, one launch (start us, length us, event | category | flops | bytes accessed | tf_op | source)
XLA Modules:
  0.0 149.7 jit_solution(3815490610961850263)
XLA Ops:
  7.2 6.1 %convolution_bitcast_fusion.1 = f32[2048,1,256]{2,0,1:T(8,128)S(1)} fusion(bf16[2048,2048]{1,0:T(8,128)(2,1)} %param.11, bf16[3,2048,256]{2,1,0:T(8,128)(2,1)} %param.19), kind=kOutput, calls=%fused_computation.6 | convolution fusion | flops 2147483648 | bytes 11534336 | tf_op jit(solution)/shard_map/dot_general | solution.py:82
  13.3 0.9 copy-done.6
  14.2 2.5 %convolution_bitcast_fusion.2 = f32[2048,1,256]{2,0,1:T(8,128)S(1)} fusion(bf16[2048,2048]{1,0:T(8,128)(2,1)S(1)} %copy-done.6, bf16[3,2048,256]{2,1,0:T(8,128)(2,1)S(1)} %copy-done.3), kind=kOutput, calls=%fused_computation.7 | convolution fusion | flops 2147483648 | bytes 11534336 | tf_op jit(solution)/shard_map/dot_general | solution.py:81
  16.8 2.4 %convolution_bitcast_fusion = f32[2048,1,256]{2,0,1:T(8,128)S(1)} fusion(bf16[2048,2048]{1,0:T(8,128)(2,1)S(1)} %bitcast.55, bf16[3,2048,256]{2,1,0:T(8,128)(2,1)S(1)} %copy-done.3), kind=kOutput, calls=%fused_computation.5 | convolution fusion | flops 2147483648 | bytes 11534336 | tf_op jit(solution)/shard_map/dot_general | solution.py:83
  21.1 1.4 fusion.1
  22.5 1.3 fusion.5
  23.9 18.0 %all_to_all.10 = bf16[16,16,3,256]{3,1,2,0:T(8,128)(2,1)S(1)} all-to-all(bf16[16,16,3,256]{3,1,2,0:T(8,128)(2,1)S(1)} %copy.47), channel_id=1, replica_groups=mesh['fs_0'=4,'fs_1'=4,'tp_0'=4,'tp_1'=2] {'fs_0','fs_1'}, dimensions={0} | all-to-all | bytes 786432 | tf_op jit(solution)/shard_map/all_to_all | solution.py:20
  42.6 1.0 broadcast_in_dim.4
  43.6 3.6 %all-to-all-start.1 = ((f32[16,16,3,256]{3,1,2,0:T(8,128)}), f32[16,16,3,256]{3,1,2,0:T(8,128)S(1)}, u32[]{:S(2)}, u32[]{:S(2)}) async-start(f32[16,16,3,256]{3,1,2,0:T(8,128)} %broadcast_in_dim.4), calls=%async_computation.1 | async-start | bytes 1572864 | tf_op jit(solution)/shard_map/all_to_all | solution.py:32
  47.3 14.0 %psum.28 = f32[3]{0:T(128)S(1)} all-reduce(f32[3]{0:T(128)S(1)} %get-tuple-element.51), channel_id=1, replica_groups=mesh['fs_0'=4,'fs_1'=4,'tp_0'=4,'tp_1'=2] {'fs_0'}, use_global_device_ids=true, to_apply=%region_2.0 | all-reduce | flops 3 | bytes 24 | tf_op jit(solution)/shard_map/psum | solution.py:40
  61.4 10.5 %psum.29 = f32[3]{0:T(128)S(1)} all-reduce(f32[3]{0:T(128)S(1)} %psum.28), channel_id=1, replica_groups=mesh['fs_0'=4,'fs_1'=4,'tp_0'=4,'tp_1'=2] {'fs_1'}, use_global_device_ids=true, to_apply=%region_3.0 | all-reduce | flops 3 | bytes 24 | tf_op jit(solution)/shard_map/psum | solution.py:40
  72.0 10.7 %psum.30 = f32[3]{0:T(128)S(1)} all-reduce(f32[3]{0:T(128)S(1)} %psum.29), channel_id=1, replica_groups=mesh['fs_0'=4,'fs_1'=4,'tp_0'=4,'tp_1'=2] {'tp_0'}, use_global_device_ids=true, to_apply=%region_4.0 | all-reduce | flops 3 | bytes 24 | tf_op jit(solution)/shard_map/psum | solution.py:40
  82.7 2.5 %psum.31 = f32[3]{0:T(128)S(1)} all-reduce(f32[3]{0:T(128)S(1)} %psum.30), channel_id=1, replica_groups=mesh['fs_0'=4,'fs_1'=4,'tp_0'=4,'tp_1'=2] {'tp_1'}, use_global_device_ids=true, to_apply=%region_5.0 | all-reduce | flops 3 | bytes 24 | tf_op jit(solution)/shard_map/psum | solution.py:40
  85.4 1.2 fusion.16
  86.7 1.2 fusion.7
  87.9 0.7 convert_bitcast_fusion
  89.4 0.8 copy.53
  90.2 0.8 copy.54
  91.0 0.8 copy.57
  91.7 0.8 copy.58
  92.5 44.7 %all-gather.2.cloned.1.call-done = bf16[2048,768]{0,1:T(8,128)(2,1)} async-done(((bf16[128,768]{0,1:T(8,128)(2,1)}), bf16[2048,768]{0,1:T(8,128)(2,1)}) %all-gather.2.cloned.1.call-update) | async-done | bytes 3145744 | tf_op jit(solution)/shard_map/all_gather | solution.py:46
  137.2 3.1 %slice_bitcast_fusion = (bf16[256,2048]{1,0:T(8,128)(2,1)}, bf16[2048,256]{0,1:T(8,128)(2,1)S(1)}, bf16[2048,256]{0,1:T(8,128)(2,1)S(1)}) fusion(bf16[2048,768]{0,1:T(8,128)(2,1)} %all-gather.2.cloned.1.call-done), kind=kLoop, calls=%fused_computation.15 | loop fusion | bytes 6291456 | tf_op jit(solution)/shard_map/transpose | solution.py:49
  140.3 1.3 copy.55
  141.6 1.3 copy.56
  (40 shorter events, 4.0 us)
Async XLA Ops:
  7.2 6.2 %copy-start.3 = (bf16[3,2048,256]{2,1,0:T(8,128)(2,1)S(1)}, bf16[3,2048,256]{2,1,0:T(8,128)(2,1)}, u32[]{:S(2)}) copy-start(bf16[3,2048,256]{2,1,0:T(8,128)(2,1)} %param.19) | copy-start | bytes 9437188
  7.2 7.0 %copy-start.6 = (bf16[2048,2048]{1,0:T(8,128)(2,1)S(1)}, bf16[2048,2048]{1,0:T(8,128)(2,1)}, u32[]{:S(2)}) copy-start(bf16[2048,2048]{1,0:T(8,128)(2,1)} %param.11) | copy-start | bytes 25165828
  7.2 9.5 %slice-start = ((s8[8388608]{0:T(1024)(128)(4,1)}), s8[4194304]{0:T(1024)(128)(4,1)S(1)}, s32[]{:S(2)}) async-start(s8[8388608]{0:T(1024)(128)(4,1)} %bitcast.54), calls=%async_computation.3 | async-start | bytes 8388608
  14.2 2.6 %slice-start.1 = ((s8[8388608]{0:T(1024)(128)(4,1)}), s8[4194304]{0:T(1024)(128)(4,1)S(1)}, s32[]{:S(2)}) async-start(s8[8388608]{0:T(1024)(128)(4,1)} %bitcast.54), calls=%async_computation.4 | async-start | bytes 8388608
  19.2 1.2 copy-start.7
  19.2 1.5 %copy-start.8 = (bf16[2048,256]{1,0:T(8,128)(2,1)S(1)}, bf16[2048,256]{1,0:T(8,128)(2,1)}, u32[]{:S(2)}) copy-start(bf16[2048,256]{1,0:T(8,128)(2,1)} %param.13) | copy-start | bytes 3145732
  19.2 1.8 %copy-start.9 = (bf16[2048,256]{1,0:T(8,128)(2,1)S(1)}, bf16[2048,256]{1,0:T(8,128)(2,1)}, u32[]{:S(2)}) copy-start(bf16[2048,256]{1,0:T(8,128)(2,1)} %param.12) | copy-start | bytes 3145732
  22.5 19.5 %copy-start.4 = (f32[16,3,256]{2,0,1:T(8,128)S(1)}, f32[16,3,256]{2,0,1:T(8,128)}, u32[]{:S(2)}) copy-start(f32[16,3,256]{2,0,1:T(8,128)} %param.21) | copy-start | bytes 147460
  22.5 19.5 %copy-start.5 = (f32[16,3,256]{2,0,1:T(8,128)S(1)}, f32[16,3,256]{2,0,1:T(8,128)}, u32[]{:S(2)}) copy-start(f32[16,3,256]{2,0,1:T(8,128)} %param.20) | copy-start | bytes 147460
  23.8 37.5 %copy-start = (f32[128,256]{1,0:T(8,128)S(1)}, f32[128,256]{1,0:T(8,128)}, u32[]{:S(2)}) copy-start(f32[128,256]{1,0:T(8,128)} %param.16) | copy-start | bytes 393220
  23.8 48.1 %copy-start.1 = (f32[128,256]{1,0:T(8,128)S(1)}, f32[128,256]{1,0:T(8,128)}, u32[]{:S(2)}) copy-start(f32[128,256]{1,0:T(8,128)} %param.17) | copy-start | bytes 393220
  43.6 41.6 %all-to-all-start.1 = ((f32[16,16,3,256]{3,1,2,0:T(8,128)}), f32[16,16,3,256]{3,1,2,0:T(8,128)S(1)}, u32[]{:S(2)}, u32[]{:S(2)}) async-start(f32[16,16,3,256]{3,1,2,0:T(8,128)} %broadcast_in_dim.4), calls=%async_computation.1 | async-start | bytes 1572864 | tf_op jit(solution)/shard_map/all_to_all | solution.py:32
  47.2 90.0 %all-gather.2.cloned.1.call-start = ((), (), s32[]{:S(2)}) async-start(), calls=%async_computation.2 | async-start | bytes 3342336 | tf_op jit(solution)/shard_map/all_gather | solution.py:46
  85.2 2.7 %copy-start.2 = (f32[256,128]{1,0:T(8,128)S(1)}, f32[256,128]{1,0:T(8,128)}, u32[]{:S(2)}) copy-start(f32[256,128]{1,0:T(8,128)} %param.18) | copy-start | bytes 393220
Sparse Core Ops, SparseCore 0:
  89.5 47.5 all-gather.1
where the time goes:
time: 150 us
  blocking collectives  55.7 us (37%)
  waiting for transfers between devices  44.7 us (30%)
  matrix products  16.1 us (11%)
  between operations  14.3 us (10%)
  local copies, waits for them, and re-layouts  12.2 us (8%)
  starting transfers between devices  3.66 us (2%)
  other arithmetic  2.94 us (2%)
    all_gather x1, waiting for transfers between devices, gather_turned(): lax.all_gather(both, axis, axis=0, tiled=True)  44.7 us
    psum x4, blocking collectives, over_axes(): return functools.reduce(lax.psum, axes, value)  37.7 us
    all_to_all x1, blocking collectives, sum_at_owner(): lax.all_to_all(pieces, axis, split_axis=0, concat_axis=0, tiled=True)  18 us
    unnamed x32, local copies, waits for them, and re-layouts  8.06 us
    dot_general x1, matrix products, on_device(): jnp.dot(normed_input, bases[1], preferred_element_type=jnp.float32)  6.11 us
    all_to_all x1, starting transfers between devices, sent_to_all(): return lax.all_to_all(copies, axis, split_axis=0, concat_axis=0, tiled=True)  3.61 us
    transpose x1, local copies, waits for them, and re-layouts, gather_turned(): finished.append(jnp.moveaxis(piece, 0, dim))  3.11 us
  transfers between devices with their start and end apart: 2, of which 1 were waited for; matrix products, arithmetic and copies ran while one was open for 2% of the time, Pallas kernels for 0%

commit v1 on v0

--- a/solution.py
+++ b/solution.py
@@ -43,7 +43,19 @@
 def gather_turned(arrays, axis, dims):
     turned = [jnp.moveaxis(a, dim, 0) for a, dim in zip(arrays, dims)]
     both = jnp.concatenate([t.reshape(len(t), -1) for t in turned], axis=1)
-    result, at, finished = (lax.all_gather(both, axis, axis=0, tiled=True), 0, [])
+    result, at, finished = (
+        jnp.concatenate(
+            lax.all_to_all(
+                jnp.stack([both for _ in range(lax.axis_size(axis))]),
+                axis_name=axis,
+                concat_axis=0,
+                split_axis=0,
+            ),
+            0,
+        ),
+        0,
+        [],
+    )
     for t, dim in zip(turned, dims):
         piece = result[:, at : at + t[0].size].reshape(-1, *t.shape[1:])
         finished.append(jnp.moveaxis(piece, 0, dim))

time: 150 us -> 146 us (0.973)
  between operations: 14.3 us -> 0.91 us
  local copies, waits for them, and re-layouts: 12.2 us -> 20.7 us
  starting transfers between devices: 3.66 us -> 7.36 us
  waiting for transfers between devices: 44.7 us -> 41.7 us
    all_gather x1 -> x0, waiting for transfers between devices: 44.7 us -> none  [gather_turned(): lax.all_gather(both, axis, axis=0, tiled=True)]
    all_to_all x0 -> x1, waiting for transfers between devices: none -> 41.7 us  [gather_turned(): lax.all_to_all(jnp.stack([both for _ in range(lax.axis_size(axis))]), axi...]
    all_to_all x0 -> x1, starting transfers between devices: none -> 3.74 us  [gather_turned(): lax.all_to_all(jnp.stack([both for _ in range(lax.axis_size(axis))]), axi...]
    all_to_all x0 -> x1, local copies, waits for them, and re-layouts: none -> 2.79 us  [gather_turned(): lax.all_to_all(jnp.stack([both for _ in range(lax.axis_size(axis))]), axi...]
    unnamed x32 -> x31, local copies, waits for them, and re-layouts: 8.06 us -> 10.5 us
    another operation x0 -> x1, local copies, waits for them, and re-layouts: none -> 2.26 us  [gather_turned(): jnp.stack([both for _ in range(lax.axis_size(axis))])]
  transfers between devices with their start and end apart: 2 -> 2, of which waited for: 1 -> 1; matrix products, arithmetic and copies ran while one was open for 2% -> 5% of each run, Pallas kernels for 0% -> 0%
where the time goes in v1:
time: 146 us
  blocking collectives  56 us (38%)
  waiting for transfers between devices  41.7 us (29%)
  local copies, waits for them, and re-layouts  20.7 us (14%)
  matrix products  16.1 us (11%)
  starting transfers between devices  7.36 us (5%)
  other arithmetic  2.96 us (2%)
    all_to_all x1, waiting for transfers between devices, gather_turned(): lax.all_to_all(jnp.stack([both for _ in range(lax.axis_size(axis))]), axi...  41.7 us
    psum x4, blocking collectives, over_axes(): return functools.reduce(lax.psum, axes, value)  38 us
    all_to_all x1, blocking collectives, sum_at_owner(): lax.all_to_all(pieces, axis, split_axis=0, concat_axis=0, tiled=True)  18 us
    unnamed x31, local copies, waits for them, and re-layouts  10.5 us
    dot_general x1, matrix products, on_device(): jnp.dot(normed_input, bases[1], preferred_element_type=jnp.float32)  6.11 us
    all_to_all x1, starting transfers between devices, gather_turned(): lax.all_to_all(jnp.stack([both for _ in range(lax.axis_size(axis))]), axi...  3.74 us
    all_to_all x1, starting transfers between devices, sent_to_all(): return lax.all_to_all(copies, axis, split_axis=0, concat_axis=0, tiled=True)  3.61 us
    transpose x1, local copies, waits for them, and re-layouts, gather_turned(): finished.append(jnp.moveaxis(piece, 0, dim))  3.41 us
  transfers between devices with their start and end apart: 2, of which 1 were waited for; matrix products, arithmetic and copies ran while one was open for 5% of the time, Pallas kernels for 0%

profile of v1, /device:TPU:0, one launch (start us, length us, event | category | flops | bytes accessed | tf_op | source)
XLA Modules:
  0.0 145.8 jit_solution(774191283561381405)
XLA Ops:
  0.7 6.1 %convolution_bitcast_fusion.1 = f32[2048,1,256]{2,0,1:T(8,128)S(1)} fusion(bf16[2048,2048]{1,0:T(8,128)(2,1)} %param.11, bf16[3,2048,256]{2,1,0:T(8,128)(2,1)} %param.19), kind=kOutput, calls=%fused_computation.6 | convolution fusion | flops 2147483648 | bytes 11534336 | tf_op jit(solution)/shard_map/dot_general | solution.py:94
  7.7 2.5 %convolution_bitcast_fusion.2 = f32[2048,1,256]{2,0,1:T(8,128)S(1)} fusion(bf16[2048,2048]{1,0:T(8,128)(2,1)S(1)} %copy-done.6, bf16[3,2048,256]{2,1,0:T(8,128)(2,1)S(1)} %copy-done.3), kind=kOutput, calls=%fused_computation.7 | convolution fusion | flops 2147483648 | bytes 11534336 | tf_op jit(solution)/shard_map/dot_general | solution.py:93
  10.3 2.3 %convolution_bitcast_fusion = f32[2048,1,256]{2,0,1:T(8,128)S(1)} fusion(bf16[2048,2048]{1,0:T(8,128)(2,1)S(1)} %bitcast.57, bf16[3,2048,256]{2,1,0:T(8,128)(2,1)S(1)} %copy-done.3), kind=kOutput, calls=%fused_computation.5 | convolution fusion | flops 2147483648 | bytes 11534336 | tf_op jit(solution)/shard_map/dot_general | solution.py:95
  14.5 1.4 fusion.1
  16.0 1.3 fusion.5
  17.3 18.0 %all_to_all.15 = bf16[16,16,3,256]{3,1,2,0:T(8,128)(2,1)S(1)} all-to-all(bf16[16,16,3,256]{3,1,2,0:T(8,128)(2,1)S(1)} %copy.61), channel_id=1, replica_groups=mesh['fs_0'=4,'fs_1'=4,'tp_0'=4,'tp_1'=2] {'fs_0','fs_1'}, dimensions={0} | all-to-all | bytes 786432 | tf_op jit(solution)/shard_map/all_to_all | solution.py:20
  36.1 1.0 broadcast_in_dim.4
  37.1 3.6 %all-to-all-start.1 = ((f32[16,16,3,256]{3,1,2,0:T(8,128)}), f32[16,16,3,256]{3,1,2,0:T(8,128)S(1)}, u32[]{:S(2)}, u32[]{:S(2)}) async-start(f32[16,16,3,256]{3,1,2,0:T(8,128)} %broadcast_in_dim.4), calls=%async_computation.1 | async-start | bytes 1572864 | tf_op jit(solution)/shard_map/all_to_all | solution.py:32
  40.7 14.1 %psum.28 = f32[3]{0:T(128)S(1)} all-reduce(f32[3]{0:T(128)S(1)} %get-tuple-element.62), channel_id=1, replica_groups=mesh['fs_0'=4,'fs_1'=4,'tp_0'=4,'tp_1'=2] {'fs_0'}, use_global_device_ids=true, to_apply=%region_2.0 | all-reduce | flops 3 | bytes 24 | tf_op jit(solution)/shard_map/psum | solution.py:40
  54.8 10.5 %psum.29 = f32[3]{0:T(128)S(1)} all-reduce(f32[3]{0:T(128)S(1)} %psum.28), channel_id=1, replica_groups=mesh['fs_0'=4,'fs_1'=4,'tp_0'=4,'tp_1'=2] {'fs_1'}, use_global_device_ids=true, to_apply=%region_3.0 | all-reduce | flops 3 | bytes 24 | tf_op jit(solution)/shard_map/psum | solution.py:40
  65.5 10.8 %psum.30 = f32[3]{0:T(128)S(1)} all-reduce(f32[3]{0:T(128)S(1)} %psum.29), channel_id=1, replica_groups=mesh['fs_0'=4,'fs_1'=4,'tp_0'=4,'tp_1'=2] {'tp_0'}, use_global_device_ids=true, to_apply=%region_4.0 | all-reduce | flops 3 | bytes 24 | tf_op jit(solution)/shard_map/psum | solution.py:40
  76.2 2.6 %psum.31 = f32[3]{0:T(128)S(1)} all-reduce(f32[3]{0:T(128)S(1)} %psum.30), channel_id=1, replica_groups=mesh['fs_0'=4,'fs_1'=4,'tp_0'=4,'tp_1'=2] {'tp_1'}, use_global_device_ids=true, to_apply=%region_5.0 | all-reduce | flops 3 | bytes 24 | tf_op jit(solution)/shard_map/psum | solution.py:40
  79.1 1.2 fusion.16
  80.3 1.2 fusion.7
  83.1 2.3 %stack.51 = bf16[16,128,768]{1,2,0:T(8,128)(2,1)} broadcast(bf16[128,768]{0,1:T(8,128)(2,1)S(1)} %pad_maximum_fusion.10), dimensions={1,2} | broadcast | bytes 3342336 | tf_op jit(solution)/shard_map/stack | solution.py:49
  85.3 3.7 %all-to-all-start.2 = ((bf16[16,128,768]{1,2,0:T(8,128)(2,1)}), bf16[16,128,768]{1,2,0:T(8,128)(2,1)S(1)}, u32[]{:S(2)}, u32[]{:S(2)}) async-start(bf16[16,128,768]{1,2,0:T(8,128)(2,1)} %stack.51), calls=%async_computation.2 | async-start | bytes 6291456 | tf_op jit(solution)/shard_map/all_to_all | solution.py:48
  89.1 1.7 %copy.68 = f32[128,256]{1,0:T(8,128)} copy(f32[128,256]{0,1:T(8,128)} %get-tuple-element.72) | data formatting | bytes 262144
  90.7 1.7 %copy.69 = f32[128,256]{1,0:T(8,128)} copy(f32[128,256]{0,1:T(8,128)} %get-tuple-element.58) | data formatting | bytes 262144
  93.1 1.7 %copy.71 = f32[128,256]{1,0:T(8,128)} copy(f32[128,256]{0,1:T(8,128)} %get-tuple-element.70) | data formatting | bytes 262144
  94.8 1.7 %copy.72 = f32[128,256]{1,0:T(8,128)} copy(f32[128,256]{0,1:T(8,128)} %get-tuple-element.69) | data formatting | bytes 262144
  96.4 41.7 %all-to-all-done.2 = bf16[16,128,768]{1,2,0:T(8,128)(2,1)S(1)} async-done(((bf16[16,128,768]{1,2,0:T(8,128)(2,1)}), bf16[16,128,768]{1,2,0:T(8,128)(2,1)S(1)}, u32[]{:S(2)}, u32[]{:S(2)}) %all-to-all-start.2) | async-done | bytes 3145760 | tf_op jit(solution)/shard_map/all_to_all | solution.py:48
  138.1 2.8 %copy.67 = bf16[16,128,768]{2,1,0:T(8,128)(2,1)} copy(bf16[16,128,768]{1,2,0:T(8,128)(2,1)S(1)} %all-to-all-done.2) | data formatting | bytes 6291456 | tf_op jit(solution)/shard_map/all_to_all | solution.py:48
  140.9 3.4 %slice_bitcast_fusion = (bf16[256,2048]{0,1:T(8,128)(2,1)S(1)}, bf16[2048,256]{1,0:T(8,128)(2,1)}, bf16[2048,256]{1,0:T(8,128)(2,1)}) fusion(bf16[2048,768]{1,0:T(8,128)(2,1)} %bitcast.54), kind=kLoop, calls=%fused_computation.15 | loop fusion | bytes 6291456 | tf_op jit(solution)/shard_map/transpose | solution.py:61
  144.3 1.4 copy.70
  (40 shorter events, 6.2 us)
Async XLA Ops:
  0.6 6.2 %copy-start.3 = (bf16[3,2048,256]{2,1,0:T(8,128)(2,1)S(1)}, bf16[3,2048,256]{2,1,0:T(8,128)(2,1)}, u32[]{:S(2)}) copy-start(bf16[3,2048,256]{2,1,0:T(8,128)(2,1)} %param.19) | copy-start | bytes 9437188
  0.7 7.0 %copy-start.6 = (bf16[2048,2048]{1,0:T(8,128)(2,1)S(1)}, bf16[2048,2048]{1,0:T(8,128)(2,1)}, u32[]{:S(2)}) copy-start(bf16[2048,2048]{1,0:T(8,128)(2,1)} %param.11) | copy-start | bytes 25165828
  0.7 9.5 %slice-start = ((s8[8388608]{0:T(1024)(128)(4,1)}), s8[4194304]{0:T(1024)(128)(4,1)S(1)}, s32[]{:S(2)}) async-start(s8[8388608]{0:T(1024)(128)(4,1)} %bitcast.56), calls=%async_computation.3 | async-start | bytes 8388608
  7.7 2.6 %slice-start.1 = ((s8[8388608]{0:T(1024)(128)(4,1)}), s8[4194304]{0:T(1024)(128)(4,1)S(1)}, s32[]{:S(2)}) async-start(s8[8388608]{0:T(1024)(128)(4,1)} %bitcast.56), calls=%async_computation.4 | async-start | bytes 8388608
  12.6 1.2 copy-start.7
  12.7 1.5 %copy-start.8 = (bf16[2048,256]{1,0:T(8,128)(2,1)S(1)}, bf16[2048,256]{1,0:T(8,128)(2,1)}, u32[]{:S(2)}) copy-start(bf16[2048,256]{1,0:T(8,128)(2,1)} %param.13) | copy-start | bytes 3145732
  12.7 1.8 %copy-start.9 = (bf16[2048,256]{1,0:T(8,128)(2,1)S(1)}, bf16[2048,256]{1,0:T(8,128)(2,1)}, u32[]{:S(2)}) copy-start(bf16[2048,256]{1,0:T(8,128)(2,1)} %param.12) | copy-start | bytes 3145732
  15.9 19.5 %copy-start.4 = (f32[16,3,256]{2,0,1:T(8,128)S(1)}, f32[16,3,256]{2,0,1:T(8,128)}, u32[]{:S(2)}) copy-start(f32[16,3,256]{2,0,1:T(8,128)} %param.21) | copy-start | bytes 147460
  16.0 19.5 %copy-start.5 = (f32[16,3,256]{2,0,1:T(8,128)S(1)}, f32[16,3,256]{2,0,1:T(8,128)}, u32[]{:S(2)}) copy-start(f32[16,3,256]{2,0,1:T(8,128)} %param.20) | copy-start | bytes 147460
  17.3 37.5 %copy-start = (f32[128,256]{1,0:T(8,128)S(1)}, f32[128,256]{1,0:T(8,128)}, u32[]{:S(2)}) copy-start(f32[128,256]{1,0:T(8,128)} %param.16) | copy-start | bytes 393220
  17.3 48.1 %copy-start.1 = (f32[128,256]{1,0:T(8,128)S(1)}, f32[128,256]{1,0:T(8,128)}, u32[]{:S(2)}) copy-start(f32[128,256]{1,0:T(8,128)} %param.17) | copy-start | bytes 393220
  37.1 41.8 %all-to-all-start.1 = ((f32[16,16,3,256]{3,1,2,0:T(8,128)}), f32[16,16,3,256]{3,1,2,0:T(8,128)S(1)}, u32[]{:S(2)}, u32[]{:S(2)}) async-start(f32[16,16,3,256]{3,1,2,0:T(8,128)} %broadcast_in_dim.4), calls=%async_computation.1 | async-start | bytes 1572864 | tf_op jit(solution)/shard_map/all_to_all | solution.py:32
  78.8 2.7 %copy-start.2 = (f32[256,128]{1,0:T(8,128)S(1)}, f32[256,128]{1,0:T(8,128)}, u32[]{:S(2)}) copy-start(f32[256,128]{1,0:T(8,128)} %param.18) | copy-start | bytes 393220
  85.3 52.8 %all-to-all-start.2 = ((bf16[16,128,768]{1,2,0:T(8,128)(2,1)}), bf16[16,128,768]{1,2,0:T(8,128)(2,1)S(1)}, u32[]{:S(2)}, u32[]{:S(2)}) async-start(bf16[16,128,768]{1,2,0:T(8,128)(2,1)} %stack.51), calls=%async_computation.2 | async-start | bytes 6291456 | tf_op jit(solution)/shard_map/all_to_all | solution.py:48
